TPU v7x, 32 devices: a whole 2x2x4 slice. The times are simulated.
32 devices in a mesh: ep: 16 (over z, x, core), tp: 2 (over y).
Axes of the slice: x: 2, y: 2, z: 4, core: 2. Of those that a mesh axis runs over, the one named last changes fastest.
Arguments:
- tokens: bfloat16 [2048, 2048], P('ep'), may hold values from -6 to 6
- routes: int32 [2048, 2], P('ep'), may hold values from 0 to 3, all different within a row; in each aligned block of 128 rows (0 to 127, 128 to 255, ...) at most 80 rows name the same one
- router_weight: bfloat16 [2048, 4], replicated, may hold values from -0.125 to 0.125
- gate_proj: bfloat16 [16, 2048, 1024], P('ep', None, 'tp'), may hold values from -0.125 to 0.125
- up_proj: bfloat16 [16, 2048, 1024], P('ep', None, 'tp'), may hold values from -0.125 to 0.125
- down_proj: bfloat16 [16, 1024, 2048], P('ep', 'tp'), may hold values from -0.09375 to 0.09375
- cotangent: bfloat16 [2048, 2048], P('ep'), may hold values from -1.5 to 1.5
Outputs:
- token_grad: bfloat16 [2048, 2048], P('ep', 'tp')
- gate_grad: float32 [2048, 2], P('ep')
- router_grad: float32 [2048, 4], P('ep')
- gate_proj_grad: float32 [16, 2048, 1024], P('ep', None, 'tp')
- up_proj_grad: float32 [16, 2048, 1024], P('ep', None, 'tp')
- down_proj_grad: float32 [16, 1024, 2048], P('ep', 'tp')
Inputs may be any that keep to these rules, and one draw needn't show every extreme that they name: `routes`: each row names 2 different experts. Among the rows of one index of ep no expert is named more than 80 times, a bound that some block reaches.
All inputs are finite; a program needn't handle non-finite values.
Results may differ from a plain program's by a relative error of at most 0.0085.
Values may be sent and summed in bfloat16 or wider, within the bound.
No kernel may reach another device: no remote copies, remote signals or barrier semaphores. Data moves between devices by JAX's collectives and lax.ppermute only.
A program may use at most 128 MiB of HBM per device.

v0:
```python
import jax
import jax.numpy as jnp
from jax import lax
from jax.sharding import PartitionSpec as P

MEMBERS = 4
TOP = 2


def shards(tokens, routes, router_weight, gate_proj, up_proj, down_proj, cotangent):
    ntok = tokens.shape[0]
    width = tokens.shape[1]
    experts = router_weight.shape[1]
    n_ep = lax.axis_size("ep")
    n_tp = lax.axis_size("tp")
    share = width // n_tp
    capacity = min(ntok, 5 * TOP * ntok // (4 * experts))
    tp_index = lax.axis_index("tp")
    logits = jnp.dot(tokens, router_weight, preferred_element_type=jnp.float32)
    onehot = (routes[:, :, None] == jnp.arange(experts, dtype=jnp.int32)[None, None, :]).astype(
        jnp.float32
    )
    chosen = jnp.sum(onehot * logits[:, None, :], axis=2)
    first = jax.nn.sigmoid(chosen[:, 0] - chosen[:, 1])
    gates = jnp.stack([first, 1.0 - first], axis=1)
    used = gates.astype(jnp.bfloat16)
    flat = onehot.reshape(ntok * TOP, experts)
    rank = jnp.cumsum(flat, axis=0) - flat
    rank_sel = jnp.sum(flat * rank, axis=1).astype(jnp.int32)
    target = routes.reshape(-1) * capacity + rank_sel
    placing = (jnp.arange(experts * capacity, dtype=jnp.int32)[:, None] == target[None, :]).astype(
        jnp.float32
    )
    place_tok = jnp.sum(placing.reshape(experts * capacity, ntok, TOP), axis=2)
    place_bf = place_tok.astype(jnp.bfloat16)

    def spread(buffer):
        tail = buffer.shape[1:]
        grown = jnp.broadcast_to(
            buffer.reshape((experts, 1, capacity) + tail), (experts, MEMBERS, capacity) + tail
        )
        return grown.reshape((n_ep * capacity,) + tail)

    gate_slots = jnp.dot(
        placing, used.reshape(-1).astype(jnp.float32), precision=lax.Precision.HIGHEST
    ).astype(jnp.bfloat16)
    gate_send = spread(gate_slots[:, None])[:, 0]
    tok_part = lax.dynamic_slice_in_dim(tokens, tp_index * share, share, 1)
    cot_part = lax.dynamic_slice_in_dim(cotangent, tp_index * share, share, 1)
    tok_send = spread(
        jnp.dot(place_bf, tok_part, preferred_element_type=jnp.float32).astype(jnp.bfloat16)
    )
    cot_send = spread(
        jnp.dot(place_bf, cot_part, preferred_element_type=jnp.float32).astype(jnp.bfloat16)
    )
    tok_half, cot_half, gate_rows = (
        lax.all_to_all(tok_send, "ep", split_axis=0, concat_axis=0, tiled=True),
        lax.all_to_all(cot_send, "ep", split_axis=0, concat_axis=0, tiled=True),
        lax.all_to_all(gate_send, "ep", split_axis=0, concat_axis=0, tiled=True),
    )
    tok_rows, cot_rows = (
        lax.all_gather(tok_half, "tp", axis=1, tiled=True),
        lax.all_gather(cot_half, "tp", axis=1, tiled=True),
    )
    w_gate = gate_proj[0]
    w_up = up_proj[0]
    w_down = down_proj[0]
    gpre = jnp.dot(tok_rows, w_gate, preferred_element_type=jnp.float32)
    upre = jnp.dot(tok_rows, w_up, preferred_element_type=jnp.float32)
    sig = jax.nn.sigmoid(gpre)
    silu_val = gpre * sig
    hidden = (silu_val * upre).astype(jnp.bfloat16)
    qvals = lax.dot_general(
        cot_rows, w_down, (((1,), (1,)), ((), ())), preferred_element_type=jnp.float32
    )
    gate_part = jnp.sum(hidden.astype(jnp.float32) * qvals, axis=1)
    weight = gate_rows.astype(jnp.float32)[:, None]
    dhid = weight * qvals
    d_gate = (dhid * upre * sig * (1.0 + gpre * (1.0 - sig))).astype(jnp.bfloat16)
    d_up = (dhid * silu_val).astype(jnp.bfloat16)
    scaled = (weight * hidden.astype(jnp.float32)).astype(jnp.bfloat16)
    grad_down = lax.dot_general(
        scaled, cot_rows, (((0,), (0,)), ((), ())), preferred_element_type=jnp.float32
    )
    grad_gate = lax.dot_general(
        tok_rows, d_gate, (((0,), (0,)), ((), ())), preferred_element_type=jnp.float32
    )
    grad_up = lax.dot_general(
        tok_rows, d_up, (((0,), (0,)), ((), ())), preferred_element_type=jnp.float32
    )
    row_grad = lax.dot_general(
        d_gate, w_gate, (((1,), (1,)), ((), ())), preferred_element_type=jnp.float32
    )
    row_grad = row_grad + lax.dot_general(
        d_up, w_up, (((1,), (1,)), ((), ())), preferred_element_type=jnp.float32
    )
    row_share = lax.psum_scatter(row_grad, "tp", scatter_dimension=1, tiled=True)
    gate_total = lax.psum(gate_part, "tp")
    back_rows, back_gate = (
        lax.all_to_all(row_share, "ep", split_axis=0, concat_axis=0, tiled=True),
        lax.all_to_all(gate_total, "ep", split_axis=0, concat_axis=0, tiled=True),
    )
    back_rows = jnp.sum(back_rows.reshape(experts, MEMBERS, capacity, share), axis=1).reshape(
        experts * capacity, share
    )
    back_gate = jnp.sum(back_gate.reshape(experts, MEMBERS, capacity), axis=1).reshape(
        experts * capacity
    )
    route_sum = lax.dot_general(
        place_tok, back_rows, (((0,), (0,)), ((), ())), precision=lax.Precision.HIGHEST
    )
    gate_grad = lax.dot_general(
        placing, back_gate, (((0,), (0,)), ((), ())), precision=lax.Precision.HIGHEST
    ).reshape(ntok, TOP)
    delta = first * (1.0 - first) * (gate_grad[:, 0] - gate_grad[:, 1])
    dlogits = delta[:, None] * (onehot[:, 0] - onehot[:, 1])
    router_rows = lax.dynamic_slice_in_dim(router_weight, tp_index * share, share, 0).astype(
        jnp.float32
    )
    router_part = lax.dot_general(
        dlogits, router_rows, (((1,), (1,)), ((), ())), precision=lax.Precision.HIGHEST
    )
    token_grad = (route_sum + router_part).astype(jnp.bfloat16)
    columns = tokens.astype(jnp.float32)
    router_grad = lax.psum_scatter(
        lax.dot_general(
            columns, dlogits, (((0,), (0,)), ((), ())), precision=lax.Precision.HIGHEST
        ),
        "ep",
        scatter_dimension=0,
        tiled=True,
    )
    return (token_grad, gate_grad, router_grad, grad_gate[None], grad_up[None], grad_down[None])


def solution(mesh):
    placed = (
        P("ep", None),
        P("ep", None),
        P(),
        P("ep", None, "tp"),
        P("ep", None, "tp"),
        P("ep", "tp", None),
        P("ep", None),
    )
    return jax.shard_map(
        shards,
        mesh=mesh,
        in_specs=placed,
        out_specs=(
            P("ep", "tp"),
            P("ep", None),
            P("ep", None),
            P("ep", None, "tp"),
            P("ep", None, "tp"),
            P("ep", "tp", None),
        ),
        check_vma=False,
    )
```

profile of v0, /device:TPU:11, one launch (start us, length us, event | category | flops | bytes accessed | tf_op | source)
XLA Modules:
  0.0 496.3 jit_solution(1121042243303813282)
XLA Ops:
  8.5 1.2 reduce-window.6
  11.1 1.3 convolution_convert_fusion
  12.8 64.9 %all_to_all.51 = bf16[16,80,1024]{2,1,0:T(8,128)(2,1)} all-to-all(bf16[16,80,1024]{2,1,0:T(8,128)(2,1)S(1)} %bitcast.86), channel_id=1, replica_groups=mesh['ep'=16,'tp'=2] {'ep'}, dimensions={0} | all-to-all | bytes 5242880 | tf_op jit(solution)/shard_map/all_to_all | solution.py:57
  79.4 63.8 %all_to_all.52 = bf16[16,80,1024]{2,1,0:T(8,128)(2,1)} all-to-all(bf16[16,80,1024]{2,1,0:T(8,128)(2,1)S(1)} %bitcast.87), channel_id=1, replica_groups=mesh['ep'=16,'tp'=2] {'ep'}, dimensions={0} | all-to-all | bytes 5242880 | tf_op jit(solution)/shard_map/all_to_all | solution.py:58
  145.1 8.4 %all_to_all.53 = bf16[16,80,1]{1,2,0:T(2,128)(2,1)S(1)} all-to-all(bf16[16,80,1]{1,2,0:T(2,128)(2,1)S(1)} %copy.64), channel_id=1, replica_groups=mesh['ep'=16,'tp'=2] {'ep'}, dimensions={0} | all-to-all | bytes 5120 | tf_op jit(solution)/shard_map/all_to_all | solution.py:59
  153.7 7.8 %fusion.5 = f32[1280,512]{0,1:T(8,128)} fusion(bf16[1280,2048]{1,0:T(8,128)(2,1)} %all-gather.5.cloned.1.call-done, bf16[1,2048,512]{2,1,0:T(8,128)(2,1)S(1)} %copy-done), kind=kOutput, calls=%fused_computation.17 | convolution fusion | flops 2684354560 | bytes 9961472 | tf_op jit(solution)/shard_map/dot_general | solution.py:68
  161.5 4.6 fusion.8
  166.1 49.9 %all-gather.3.cloned.1.call-done = bf16[1280,2048]{1,0:T(8,128)(2,1)} async-done(((bf16[1280,1024]{1,0:T(8,128)(2,1)}), bf16[1280,2048]{1,0:T(8,128)(2,1)}) %all-gather.3.cloned.1.call-update) | async-done | bytes 5242896 | tf_op jit(solution)/shard_map/all_gather | solution.py:63
  216.1 9.6 %fusion = (f32[1280]{0:T(1024)S(1)}, bf16[1280,512]{0,1:T(8,128)(2,1)}, bf16[1280,512]{0,1:T(8,128)(2,1)S(1)}, bf16[1280,512]{0,1:T(8,128)(2,1)S(1)}) fusion(f32[1280,512]{0,1:T(8,128)} %fusion.8, f32[1280,512]{0,1:T(8,128)} %fusion.5, f32[1280]{0:T(1024)S(1)} %reshape.131, bf16[1280,2048]{1,0:T(8,128)(2,1)} %all-gather.3.cloned.1.call-done, ...), kind=kOutput, calls=%fused_computation.7 | convolution fusion | flops 2696805120 | bytes 16525312 | tf_op jit(solution)/shard_map/dot_general | solution.py:73
  225.7 3.2 fusion.3
  228.9 5.6 %convolution_add_fusion = f32[1280,2048]{1,0:T(8,128)} fusion(f32[1280,2048]{1,0:T(8,128)S(1)} %fusion.3, bf16[1280,512]{0,1:T(8,128)(2,1)S(1)} %get-tuple-element.11, bf16[1,2048,512]{2,1,0:T(8,128)(2,1)S(1)} %copy-done.7), kind=kOutput, calls=%fused_computation | convolution fusion | flops 2686976000 | bytes 24379392 | tf_op jit(solution)/shard_map/dot_general | solution.py:94
  234.6 3.8 psum.7
  238.4 11.4 %all_to_all.54 = f32[16,80,1]{1,2,0:T(1,128)S(1)} all-to-all(f32[16,80,1]{1,2,0:T(1,128)S(1)} %bitcast.93), channel_id=1, replica_groups=mesh['ep'=16,'tp'=2] {'ep'}, dimensions={0} | all-to-all | bytes 10240 | tf_op jit(solution)/shard_map/all_to_all | solution.py:101
  249.8 106.8 %reduce-scatter.5.cloned.1.call-done = f32[1280,1024]{1,0:T(8,128)} async-done(((f32[1280,2048]{1,0:T(8,128)}), f32[1280,1024]{1,0:T(8,128)}) %reduce-scatter.5.cloned.1.call-update) | async-done | bytes 5242896 | tf_op jit(solution)/shard_map/reduce_scatter | solution.py:97
  356.6 6.6 %all-to-all-start.3 = ((f32[16,80,1024]{2,1,0:T(8,128)}), f32[16,80,1024]{2,1,0:T(8,128)}, u32[]{:S(2)}, u32[]{:S(2)}) async-start(f32[16,80,1024]{2,1,0:T(8,128)} %bitcast.88), calls=%async_computation.4 | async-start | bytes 10485760 | tf_op jit(solution)/shard_map/all_to_all | solution.py:100
  363.6 7.2 %convolution_bitcast_fusion.2 = f32[1,2048,512]{2,1,0:T(8,128)} fusion(bf16[1280,2048]{1,0:T(8,128)(2,1)} %all-gather.5.cloned.1.call-done, bf16[1280,512]{0,1:T(8,128)(2,1)S(1)} %copy-done.14), kind=kOutput, calls=%fused_computation.6 | convolution fusion | flops 2684354560 | bytes 10747904 | tf_op jit(solution)/shard_map/dot_general | solution.py:85
  370.9 7.2 %convolution_bitcast_fusion.1 = f32[1,2048,512]{2,1,0:T(8,128)} fusion(bf16[1280,2048]{1,0:T(8,128)(2,1)} %all-gather.5.cloned.1.call-done, bf16[1280,512]{0,1:T(8,128)(2,1)S(1)} %get-tuple-element.11), kind=kOutput, calls=%fused_computation.5 | convolution fusion | flops 2684354560 | bytes 10747904 | tf_op jit(solution)/shard_map/dot_general | solution.py:88
  378.1 4.5 convolution_bitcast_fusion
  383.4 1.4 copy.71
  385.3 85.3 %reduce-scatter.7.cloned.1.call-done = f32[128,4]{1,0:T(8,128)} async-done(((f32[2048,4]{1,0:T(8,128)}), f32[128,4]{1,0:T(8,128)}) %reduce-scatter.7.cloned.1.call-update) | async-done | bytes 2064
  470.7 1.5 copy.72
  472.2 12.4 %all-to-all-done.3 = f32[16,80,1024]{2,1,0:T(8,128)} async-done(((f32[16,80,1024]{2,1,0:T(8,128)}), f32[16,80,1024]{2,1,0:T(8,128)}, u32[]{:S(2)}, u32[]{:S(2)}) %all-to-all-start.3) | async-done | bytes 5242912 | tf_op jit(solution)/shard_map/all_to_all | solution.py:100
  484.6 3.3 bitcast_reduce_fusion
  487.9 1.8 fusion.14
  (90 shorter events, 8.4 us)
Async XLA Ops:
  7.2 146.5 %copy-start = (bf16[1,2048,512]{2,1,0:T(8,128)(2,1)S(1)}, bf16[1,2048,512]{2,1,0:T(8,128)(2,1)}, u32[]{:S(2)}) copy-start(bf16[1,2048,512]{2,1,0:T(8,128)(2,1)} %param.10) | copy-start | bytes 6291460
  7.2 146.5 %all-gather.5.cloned.1.call-start = ((), (), s32[]{:S(2)}) async-start(), calls=%async_computation.8 | async-start | bytes 7864320 | tf_op jit(solution)/shard_map/all_gather | solution.py:62
  11.1 66.7 %copy-start.4 = (f32[320,128]{1,0:T(8,128)}, f32[320,128]{1,0:T(8,128)S(1)}, u32[]{:S(2)}) copy-start(f32[320,128]{1,0:T(8,128)S(1)} %convert_reduce_fusion) | copy-start | bytes 491524
  77.7 1.0 copy-start.8
  77.7 138.4 %all-gather.3.cloned.1.call-start = ((), (), s32[]{:S(2)}) async-start(), calls=%async_computation.7 | async-start | bytes 7864320 | tf_op jit(solution)/shard_map/all_gather | solution.py:63
  143.2 1.0 copy-start.2
  143.2 1.0 copy-start.9
  143.2 1.3 copy-start.10
  143.2 213.4 %reduce-scatter.5.cloned.1.call-start = ((), (), s32[]{:S(2)}) async-start(), calls=%async_computation.9 | async-start | bytes 15728640 | tf_op jit(solution)/shard_map/reduce_scatter | solution.py:97
  153.7 7.8 %copy-start.6 = (bf16[1,2048,512]{2,1,0:T(8,128)(2,1)S(1)}, bf16[1,2048,512]{2,1,0:T(8,128)(2,1)}, u32[]{:S(2)}) copy-start(bf16[1,2048,512]{2,1,0:T(8,128)(2,1)} %param.11) | copy-start | bytes 6291460
  153.7 7.8 %copy-start.12 = (bf16[1280,2048]{1,0:T(8,128)(2,1)S(1)}, bf16[1280,2048]{1,0:T(8,128)(2,1)}, u32[]{:S(2)}) copy-start(bf16[1280,2048]{1,0:T(8,128)(2,1)} %all-gather.5.cloned.1.call-done) | copy-start | bytes 15728644
  225.7 3.2 copy-start.13
  225.7 3.2 copy-start.7
  356.6 7.0 %copy-start.14 = (bf16[1280,512]{0,1:T(8,128)(2,1)S(1)}, bf16[1280,512]{0,1:T(8,128)(2,1)}, u32[]{:S(2)}) copy-start(bf16[1280,512]{0,1:T(8,128)(2,1)} %copy-done.13) | copy-start | bytes 3932164
  356.6 127.9 %all-to-all-start.3 = ((f32[16,80,1024]{2,1,0:T(8,128)}), f32[16,80,1024]{2,1,0:T(8,128)}, u32[]{:S(2)}, u32[]{:S(2)}) async-start(f32[16,80,1024]{2,1,0:T(8,128)} %bitcast.88), calls=%async_computation.4 | async-start | bytes 10485760 | tf_op jit(solution)/shard_map/all_to_all | solution.py:100
  363.3 107.4 %reduce-scatter.7.cloned.1.call-start = ((), (), s32[]{:S(2)}) async-start(), calls=%async_computation.10 | async-start | bytes 1114112
  363.6 14.5 %slice-start = ((s8[5242880]{0:T(1024)(128)(4,1)}), s8[4194304]{0:T(1024)(128)(4,1)S(1)}, s32[]{:S(2)}) async-start(s8[5242880]{0:T(1024)(128)(4,1)} %bitcast.96), calls=%async_computation.11 | async-start | bytes 8388608
  370.9 7.2 %slice-start.1 = ((s8[5242880]{0:T(1024)(128)(4,1)}), s8[1048576]{0:T(1024)(128)(4,1)S(1)}, s32[]{:S(2)}) async-start(s8[5242880]{0:T(1024)(128)(4,1)} %bitcast.96), calls=%async_computation.12 | async-start | bytes 2097152
  370.9 7.2 %copy-start.15 = (bf16[1280,512]{0,1:T(8,128)(2,1)S(1)}, bf16[1280,512]{0,1:T(8,128)(2,1)}, u32[]{:S(2)}) copy-start(bf16[1280,512]{0,1:T(8,128)(2,1)} %get-tuple-element.9) | copy-start | bytes 3932164
  378.1 5.0 %copy-start.3 = (bf16[128,2048]{1,0:T(8,128)(2,1)S(1)}, bf16[128,2048]{1,0:T(8,128)(2,1)}, u32[]{:S(2)}) copy-start(bf16[128,2048]{1,0:T(8,128)(2,1)} %param.7) | copy-start | bytes 1572868
  383.1 104.8 %copy-start.11 = (f32[128,2]{0,1:T(2,128)}, f32[128,2]{0,1:T(2,128)S(1)}, u32[]{:S(2)}) copy-start(f32[128,2]{0,1:T(2,128)S(1)} %copy.70) | copy-start | bytes 3076
  472.2 15.8 %copy-start.5 = (f32[320,128]{1,0:T(8,128)S(1)}, f32[320,128]{1,0:T(8,128)}, u32[]{:S(2)}) copy-start(f32[320,128]{1,0:T(8,128)} %copy-done.4) | copy-start | bytes 491524
  484.6 5.2 %copy-start.1 = (bf16[1,2048,512]{2,1,0:T(8,128)(2,1)S(1)}, bf16[1,2048,512]{2,1,0:T(8,128)(2,1)}, u32[]{:S(2)}) copy-start(bf16[1,2048,512]{2,1,0:T(8,128)(2,1)} %param.10) | copy-start | bytes 6291460
Sparse Core Ops, SparseCore 0:
  77.8 68.0 all-gather.4
  147.5 68.5 all-gather.2
  234.7 121.9 reduce-scatter.4
  385.0 85.6 reduce-scatter.6
where the time goes:
time: 497 us; the launch traced here: 496 us
  waiting for transfers between devices  255 us (51%)
  blocking collectives  152 us (31%)
  matrix products  54.4 us (11%)
  between operations  14.1 us (3%)
  local copies, waits for them, and re-layouts  8.03 us (2%)
  starting transfers between devices  6.8 us (1%)
  other arithmetic  6.04 us (1%)
    reduce_scatter x1, waiting for transfers between devices, shards(): lax.psum_scatter(row_grad, 'tp', scatter_dimension=1, tiled=True)  107 us
    unnamed x5, waiting for transfers between devices  85.4 us
    all_to_all x1, blocking collectives, shards(): lax.all_to_all(tok_send, 'ep', split_axis=0, concat_axis=0, tiled=True)  64.9 us
    all_to_all x1, blocking collectives, shards(): lax.all_to_all(cot_send, 'ep', split_axis=0, concat_axis=0, tiled=True)  63.8 us
    all_gather x1, waiting for transfers between devices, shards(): lax.all_gather(cot_half, 'tp', axis=1, tiled=True)  49.9 us
    all_to_all x1, waiting for transfers between devices, shards(): lax.all_to_all(row_share, 'ep', split_axis=0, concat_axis=0, tiled=True)  12.4 us
    all_to_all x1, blocking collectives, shards(): lax.all_to_all(gate_total, 'ep', split_axis=0, concat_axis=0, tiled=True)  11.4 us
  transfers between devices with their start and end apart: 5, of which 4 were waited for; matrix products, arithmetic and copies ran while one was open for 8% of the time, Pallas kernels for 0%

commit v1 on v0

--- a/solution.py
+++ b/solution.py
@@ -5,6 +5,13 @@
 
 MEMBERS = 4
 TOP = 2
+
+
+def exchange_gather(x, name, d):
+    count = lax.axis_size(name)
+    blocks = jnp.stack([x for _ in range(count)])
+    blocks = lax.all_to_all(blocks, name, split_axis=0, concat_axis=0)
+    return jnp.concatenate(blocks, axis=d)
 
 
 def shards(tokens, routes, router_weight, gate_proj, up_proj, down_proj, cotangent):
@@ -60,7 +67,7 @@
     )
     tok_rows, cot_rows = (
         lax.all_gather(tok_half, "tp", axis=1, tiled=True),
-        lax.all_gather(cot_half, "tp", axis=1, tiled=True),
+        exchange_gather(cot_half, "tp", 1),
     )
     w_gate = gate_proj[0]
     w_up = up_proj[0]

time: 497 us -> 513 us (1.032)
  blocking collectives: 152 us -> 15.6 us
  waiting for transfers between devices: 255 us -> 378 us
  starting transfers between devices: 6.8 us -> 28.5 us
  local copies, waits for them, and re-layouts: 8.03 us -> 18 us
  matrix products: 54.4 us -> 46.9 us
  other arithmetic: 6.04 us -> 11.4 us
    all_to_all x0 -> x4, waiting for transfers between devices: none -> 173 us  [the longest x1 58.4 us: shards(): lax.all_to_all(tok_send, 'ep', split_axis=0, concat_axis=0, tiled=True)]
    all_to_all x3 -> x0, blocking collectives: 137 us -> none  [the longest x1 64.9 us: shards(): lax.all_to_all(tok_send, 'ep', split_axis=0, concat_axis=0, tiled=True)]
    all_gather x1 -> x0, waiting for transfers between devices: 49.9 us -> none  [shards(): lax.all_gather(cot_half, 'tp', axis=1, tiled=True)]
    all_to_all x0 -> x4, starting transfers between devices: none -> 21.9 us  [the longest x1 6.65 us: shards(): lax.all_to_all(tok_send, 'ep', split_axis=0, concat_axis=0, tiled=True)]
    reshape x0 -> x1, local copies, waits for them, and re-layouts: none -> 7.96 us  [exchange_gather(): return jnp.concatenate(blocks, axis=d)]
    another operation x4 -> x5, other arithmetic: 1.28 us -> 6.59 us  [the longest x1 5.31 us: exchange_gather(): blocks = jnp.stack([x for _ in range(count)])]
    unnamed x5 -> x4, waiting for transfers between devices: 85.4 us -> 85.6 us
  transfers between devices with their start and end apart: 5 -> 8, of which waited for: 4 -> 6; matrix products, arithmetic and copies ran while one was open for 8% -> 8% of each run, Pallas kernels for 0% -> 0%
where the time goes in v1:
time: 513 us; the launch traced here: 512 us
  waiting for transfers between devices  378 us (74%)
  matrix products  46.9 us (9%)
  starting transfers between devices  28.5 us (6%)
  local copies, waits for them, and re-layouts  18 us (4%)
  blocking collectives  15.6 us (3%)
  between operations  14.1 us (3%)
  other arithmetic  11.4 us (2%)
    reduce_scatter x1, waiting for transfers between devices, shards(): lax.psum_scatter(row_grad, 'tp', scatter_dimension=1, tiled=True)  107 us
    unnamed x4, waiting for transfers between devices  85.6 us
    all_to_all x1, waiting for transfers between devices, shards(): lax.all_to_all(tok_send, 'ep', split_axis=0, concat_axis=0, tiled=True)  58.4 us
    all_to_all x1, waiting for transfers between devices, exchange_gather(): blocks = lax.all_to_all(blocks, name, split_axis=0, concat_axis=0)  58.2 us
    all_to_all x1, waiting for transfers between devices, shards(): lax.all_to_all(cot_send, 'ep', split_axis=0, concat_axis=0, tiled=True)  56.5 us
    all_to_all x1, waiting for transfers between devices, shards(): lax.all_to_all(row_share, 'ep', split_axis=0, concat_axis=0, tiled=True)  12.2 us
    all_to_all x1, blocking collectives, shards(): lax.all_to_all(gate_total, 'ep', split_axis=0, concat_axis=0, tiled=True)  11.7 us
  transfers between devices with their start and end apart: 8, of which 6 were waited for; matrix products, arithmetic and copies ran while one was open for 8% of the time, Pallas kernels for 0%

profile of v1, /device:TPU:11, one launch (start us, length us, event | category | flops | bytes accessed | tf_op | source)
XLA Modules:
  0.0 512.0 jit_solution(17560177971899138219)
XLA Ops:
  14.2 6.7 %all-to-all-start.3 = ((bf16[16,80,1024]{2,1,0:T(8,128)(2,1)}), bf16[16,80,1024]{2,1,0:T(8,128)(2,1)}, u32[]{:S(2)}, u32[]{:S(2)}) async-start(bf16[16,80,1024]{2,1,0:T(8,128)(2,1)} %bitcast.87), calls=%async_computation.3 | async-start | bytes 5242880 | tf_op jit(solution)/shard_map/all_to_all | solution.py:64
  21.2 58.4 %all-to-all-done.3 = bf16[16,80,1024]{2,1,0:T(8,128)(2,1)} async-done(((bf16[16,80,1024]{2,1,0:T(8,128)(2,1)}), bf16[16,80,1024]{2,1,0:T(8,128)(2,1)}, u32[]{:S(2)}, u32[]{:S(2)}) %all-to-all-start.3) | async-done | bytes 2621472 | tf_op jit(solution)/shard_map/all_to_all | solution.py:64
  81.4 4.8 all-to-all-start.1
  88.8 56.5 %all-to-all-done.1 = bf16[16,80,1024]{2,1,0:T(8,128)(2,1)} async-done(((bf16[16,80,1024]{2,1,0:T(8,128)(2,1)}), bf16[16,80,1024]{2,1,0:T(8,128)(2,1)}, u32[]{:S(2)}, u32[]{:S(2)}) %all-to-all-start.1) | async-done | bytes 2621472 | tf_op jit(solution)/shard_map/all_to_all | solution.py:65
  145.3 4.5 all-to-all-start
  149.8 5.3 %pad_maximum_fusion = bf16[2,1280,1024]{2,1,0:T(8,128)(2,1)} fusion(bf16[1,1280,1024]{2,1,0:T(8,128)(2,1)} %bitcast.6), kind=kLoop, calls=%fused_computation.1 | loop fusion | flops 2621440 | bytes 7864320 | tf_op jit(solution)/shard_map/stack | solution.py:12
  155.1 5.9 %all-to-all-start.2 = ((bf16[2,1280,1024]{2,1,0:T(8,128)(2,1)}), bf16[2,1280,1024]{2,1,0:T(8,128)(2,1)}, u32[]{:S(2)}, u32[]{:S(2)}) async-start(bf16[2,1280,1024]{2,1,0:T(8,128)(2,1)} %pad_maximum_fusion), calls=%async_computation.2 | async-start | bytes 10485760 | tf_op jit(solution)/shard_map/all_to_all | solution.py:13
  161.2 58.2 %all-to-all-done.2 = bf16[2,1280,1024]{2,1,0:T(8,128)(2,1)} async-done(((bf16[2,1280,1024]{2,1,0:T(8,128)(2,1)}), bf16[2,1280,1024]{2,1,0:T(8,128)(2,1)}, u32[]{:S(2)}, u32[]{:S(2)}) %all-to-all-start.2) | async-done | bytes 5242912 | tf_op jit(solution)/shard_map/all_to_all | solution.py:13
  219.3 8.0 %copy.79 = bf16[1280,2,1024]{0,2,1:T(8,128)(2,1)} copy(bf16[1280,2,1024]{2,0,1:T(8,128)(2,1)} %bitcast.7) | data formatting | bytes 10485760 | tf_op jit(solution)/shard_map/reshape | solution.py:14
  227.3 5.7 %fusion.5 = f32[1280,512]{0,1:T(8,128)S(1)} fusion(bf16[1280,2048]{1,0:T(8,128)(2,1)} %all-gather.2.cloned.1.call-done, bf16[1,2048,512]{2,1,0:T(8,128)(2,1)S(1)} %copy-done), kind=kOutput, calls=%fused_computation.18 | convolution fusion | flops 2684354560 | bytes 9961472 | tf_op jit(solution)/shard_map/dot_general | solution.py:75
  233.1 3.2 fusion.8
  236.3 5.0 fusion
  241.3 2.9 fusion.3
  244.3 5.8 %convolution_add_fusion = f32[1280,2048]{1,0:T(8,128)} fusion(f32[1280,2048]{1,0:T(8,128)S(1)} %fusion.3, bf16[1280,512]{0,1:T(8,128)(2,1)S(1)} %get-tuple-element.11, bf16[1,2048,512]{2,1,0:T(8,128)(2,1)S(1)} %copy-done.6), kind=kOutput, calls=%fused_computation | convolution fusion | flops 2686976000 | bytes 24379392 | tf_op jit(solution)/shard_map/dot_general | solution.py:101
  250.2 3.8 psum.7
  254.0 11.7 %all_to_all.53 = f32[16,80,1]{1,2,0:T(1,128)S(1)} all-to-all(f32[16,80,1]{1,2,0:T(1,128)S(1)} %bitcast.99), channel_id=1, replica_groups=mesh['ep'=16,'tp'=2] {'ep'}, dimensions={0} | all-to-all | bytes 10240 | tf_op jit(solution)/shard_map/all_to_all | solution.py:108
  265.7 106.8 %reduce-scatter.5.cloned.1.call-done = f32[1280,1024]{1,0:T(8,128)} async-done(((f32[1280,2048]{1,0:T(8,128)}), f32[1280,1024]{1,0:T(8,128)}) %reduce-scatter.5.cloned.1.call-update) | async-done | bytes 5242896 | tf_op jit(solution)/shard_map/reduce_scatter | solution.py:104
  372.6 6.5 %all-to-all-start.4 = ((f32[16,80,1024]{2,1,0:T(8,128)}), f32[16,80,1024]{2,1,0:T(8,128)}, u32[]{:S(2)}, u32[]{:S(2)}) async-start(f32[16,80,1024]{2,1,0:T(8,128)} %bitcast.88), calls=%async_computation.5 | async-start | bytes 10485760 | tf_op jit(solution)/shard_map/all_to_all | solution.py:107
  379.4 8.0 %convolution_bitcast_fusion.2 = f32[1,2048,512]{2,1,0:T(8,128)} fusion(bf16[1280,2048]{1,0:T(8,128)(2,1)} %all-gather.2.cloned.1.call-done, bf16[1280,512]{0,1:T(8,128)(2,1)} %copy-done.13), kind=kOutput, calls=%fused_computation.7 | convolution fusion | flops 2684354560 | bytes 10747904 | tf_op jit(solution)/shard_map/dot_general | solution.py:92
  387.4 7.2 %convolution_bitcast_fusion.1 = f32[1,2048,512]{2,1,0:T(8,128)} fusion(bf16[1280,2048]{1,0:T(8,128)(2,1)} %all-gather.2.cloned.1.call-done, bf16[1280,512]{0,1:T(8,128)(2,1)S(1)} %get-tuple-element.11), kind=kOutput, calls=%fused_computation.6 | convolution fusion | flops 2684354560 | bytes 10747904 | tf_op jit(solution)/shard_map/dot_general | solution.py:95
  394.6 4.5 convolution_bitcast_fusion
  401.8 84.9 %reduce-scatter.7.cloned.1.call-done = f32[128,4]{1,0:T(8,128)} async-done(((f32[2048,4]{1,0:T(8,128)}), f32[128,4]{1,0:T(8,128)}) %reduce-scatter.7.cloned.1.call-update) | async-done | bytes 2064
  488.2 12.2 %all-to-all-done.4 = f32[16,80,1024]{2,1,0:T(8,128)} async-done(((f32[16,80,1024]{2,1,0:T(8,128)}), f32[16,80,1024]{2,1,0:T(8,128)}, u32[]{:S(2)}, u32[]{:S(2)}) %all-to-all-start.4) | async-done | bytes 5242912 | tf_op jit(solution)/shard_map/all_to_all | solution.py:107
  500.4 3.3 bitcast_reduce_fusion
  (97 shorter events, 18.2 us)
Async XLA Ops:
  7.2 220.2 %copy-start = (bf16[1,2048,512]{2,1,0:T(8,128)(2,1)S(1)}, bf16[1,2048,512]{2,1,0:T(8,128)(2,1)}, u32[]{:S(2)}) copy-start(bf16[1,2048,512]{2,1,0:T(8,128)(2,1)} %param.10) | copy-start | bytes 6291460
  11.0 9.8 %copy-start.4 = (f32[320,128]{1,0:T(8,128)}, f32[320,128]{1,0:T(8,128)S(1)}, u32[]{:S(2)}) copy-start(f32[320,128]{1,0:T(8,128)S(1)} %convert_reduce_fusion) | copy-start | bytes 491524
  14.2 6.7 %copy-start.7 = (bf16[128,2048]{1,0:T(8,128)(2,1)S(1)}, bf16[128,2048]{1,0:T(8,128)(2,1)}, u32[]{:S(2)}) copy-start(bf16[128,2048]{1,0:T(8,128)(2,1)} %param.13) | copy-start | bytes 1572868
  14.2 65.4 %all-to-all-start.3 = ((bf16[16,80,1024]{2,1,0:T(8,128)(2,1)}), bf16[16,80,1024]{2,1,0:T(8,128)(2,1)}, u32[]{:S(2)}, u32[]{:S(2)}) async-start(bf16[16,80,1024]{2,1,0:T(8,128)(2,1)} %bitcast.87), calls=%async_computation.3 | async-start | bytes 5242880 | tf_op jit(solution)/shard_map/all_to_all | solution.py:64
  81.4 63.8 %all-to-all-start.1 = ((bf16[16,80,1024]{2,1,0:T(8,128)(2,1)}), bf16[16,80,1024]{2,1,0:T(8,128)(2,1)}, u32[]{:S(2)}, u32[]{:S(2)}) async-start(bf16[16,80,1024]{2,1,0:T(8,128)(2,1)} %bitcast.86), calls=%async_computation.1 | async-start | bytes 5242880 | tf_op jit(solution)/shard_map/all_to_all | solution.py:65
  86.3 141.1 %all-gather.2.cloned.1.call-start = ((), (), s32[]{:S(2)}) async-start(), calls=%async_computation.8 | async-start | bytes 7864320 | tf_op jit(solution)/shard_map/all_gather | solution.py:69
  145.3 9.8 %all-to-all-start = ((bf16[16,80,1]{1,2,0:T(2,128)(2,1)}), bf16[16,80,1]{1,2,0:T(2,128)(2,1)S(1)}, u32[]{:S(2)}, u32[]{:S(2)}) async-start(bf16[16,80,1]{1,2,0:T(2,128)(2,1)} %copy.78), calls=%async_computation | async-start | bytes 16384 | tf_op jit(solution)/shard_map/all_to_all | solution.py:66
  155.1 64.3 %all-to-all-start.2 = ((bf16[2,1280,1024]{2,1,0:T(8,128)(2,1)}), bf16[2,1280,1024]{2,1,0:T(8,128)(2,1)}, u32[]{:S(2)}, u32[]{:S(2)}) async-start(bf16[2,1280,1024]{2,1,0:T(8,128)(2,1)} %pad_maximum_fusion), calls=%async_computation.2 | async-start | bytes 10485760 | tf_op jit(solution)/shard_map/all_to_all | solution.py:13
  161.0 211.5 %reduce-scatter.5.cloned.1.call-start = ((), (), s32[]{:S(2)}) async-start(), calls=%async_computation.9 | async-start | bytes 15728640 | tf_op jit(solution)/shard_map/reduce_scatter | solution.py:104
  227.3 5.7 %copy-start.6 = (bf16[1,2048,512]{2,1,0:T(8,128)(2,1)S(1)}, bf16[1,2048,512]{2,1,0:T(8,128)(2,1)}, u32[]{:S(2)}) copy-start(bf16[1,2048,512]{2,1,0:T(8,128)(2,1)} %param.11) | copy-start | bytes 6291460
  227.3 5.7 %copy-start.11 = (bf16[1280,2048]{1,0:T(8,128)(2,1)S(1)}, bf16[1280,2048]{1,0:T(8,128)(2,1)}, u32[]{:S(2)}) copy-start(bf16[1280,2048]{1,0:T(8,128)(2,1)} %all-gather.2.cloned.1.call-done) | copy-start | bytes 15728644
  227.3 9.0 %slice-start = ((s8[5242880]{0:T(1024)(128)(4,1)}), s8[4194304]{0:T(1024)(128)(4,1)S(1)}, s32[]{:S(2)}) async-start(s8[5242880]{0:T(1024)(128)(4,1)} %bitcast.89), calls=%async_computation.11 | async-start | bytes 8388608
  233.1 3.2 slice-start.1
  233.1 3.2 copy-start.12
  241.3 2.9 copy-start.13
  372.6 127.8 %all-to-all-start.4 = ((f32[16,80,1024]{2,1,0:T(8,128)}), f32[16,80,1024]{2,1,0:T(8,128)}, u32[]{:S(2)}, u32[]{:S(2)}) async-start(f32[16,80,1024]{2,1,0:T(8,128)} %bitcast.88), calls=%async_computation.5 | async-start | bytes 10485760 | tf_op jit(solution)/shard_map/all_to_all | solution.py:107
  379.1 107.7 %reduce-scatter.7.cloned.1.call-start = ((), (), s32[]{:S(2)}) async-start(), calls=%async_computation.10 | async-start | bytes 1114112
  379.4 15.2 %slice-start.2 = ((s8[5242880]{0:T(1024)(128)(4,1)}), s8[4194304]{0:T(1024)(128)(4,1)S(1)}, s32[]{:S(2)}) async-start(s8[5242880]{0:T(1024)(128)(4,1)} %bitcast.92), calls=%async_computation.13 | async-start | bytes 8388608
  387.4 7.2 %slice-start.3 = ((s8[5242880]{0:T(1024)(128)(4,1)}), s8[1048576]{0:T(1024)(128)(4,1)S(1)}, s32[]{:S(2)}) async-start(s8[5242880]{0:T(1024)(128)(4,1)} %bitcast.92), calls=%async_computation.14 | async-start | bytes 2097152
  387.4 7.2 %copy-start.14 = (bf16[1280,512]{0,1:T(8,128)(2,1)S(1)}, bf16[1280,512]{0,1:T(8,128)(2,1)}, u32[]{:S(2)}) copy-start(bf16[1280,512]{0,1:T(8,128)(2,1)} %get-tuple-element.9) | copy-start | bytes 3932164
  394.6 5.0 copy-start.3
  399.6 104.1 %copy-start.10 = (f32[128,2]{0,1:T(2,128)}, f32[128,2]{0,1:T(2,128)S(1)}, u32[]{:S(2)}) copy-start(f32[128,2]{0,1:T(2,128)S(1)} %copy.85) | copy-start | bytes 3076
  488.2 15.5 %copy-start.5 = (f32[320,128]{1,0:T(8,128)S(1)}, f32[320,128]{1,0:T(8,128)}, u32[]{:S(2)}) copy-start(f32[320,128]{1,0:T(8,128)} %copy-done.4) | copy-start | bytes 491524
  500.4 5.1 %copy-start.1 = (bf16[1,2048,512]{2,1,0:T(8,128)(2,1)S(1)}, bf16[1,2048,512]{2,1,0:T(8,128)(2,1)}, u32[]{:S(2)}) copy-start(bf16[1,2048,512]{2,1,0:T(8,128)(2,1)} %param.10) | copy-start | bytes 6291460
  (3 other events, 3.3 us)
Sparse Core Ops, SparseCore 0:
  88.6 68.9 all-gather.1
  250.2 122.3 reduce-scatter.4
  401.5 85.1 reduce-scatter.6
